TPU v7x, 32 devices: a whole 2x2x4 slice. The times are simulated.
32 devices in a mesh: sp: 4 (over z), fs: 4 (over y, x), tp: 2 (over core).
Axes of the slice: x: 2, y: 2, z: 4, core: 2. Of those that a mesh axis runs over, the one named last changes fastest.
Arguments:
- tokens: bfloat16 [4, 1536, 2048], P('fs', ('sp', 'tp')), may hold values from -6 to 6
- norm_gain: float32 [2048], replicated, may hold values from 0.1 to 1.9
- conv_gate_w: bfloat16 [2048, 1024], P('sp', 'tp'), may hold values from -0.125 to 0.125
- conv_in_w: bfloat16 [2048, 1024], P('sp', 'tp'), may hold values from -0.125 to 0.125
- query_w: bfloat16 [2048, 1024], P('sp', 'tp'), may hold values from -0.125 to 0.125
- forget_w: bfloat16 [2048, 1024], P('sp', 'tp'), may hold values from -0.125 to 0.125
- value_w: bfloat16 [2048, 1024], P('sp', 'tp'), may hold values from -0.125 to 0.125
- conv_taps: float32 [3, 1024], P(None, 'tp'), may hold values from -3.5 to 3.5
- floor_gate: float32 [1024], P('tp'), may hold values from 0.93 to 1
- leak: float32 [4, 1536, 8], P('fs', 'sp', 'tp'), may hold values from -1.4 to 0
- head_gain: float32 [128], replicated, may hold values from 0.1 to 1.9
- conv_out_w: bfloat16 [1024, 2048], P('tp', 'fs'), may hold values from -0.125 to 0.125
- chain_out_w: bfloat16 [1024, 2048], P('tp', 'fs'), may hold values from -0.125 to 0.125
Outputs:
- mixed: bfloat16 [4, 1536, 2048], P('fs', ('sp', 'tp'))
All inputs are finite; a program needn't handle non-finite values.
Results may differ from a plain program's by a relative error of at most 0.013.
Values may be sent and summed in bfloat16 or wider, within the bound.
A program may use at most 128 MiB of HBM per device.

v0:
```python
import jax
import jax.numpy as jnp
from jax import lax
from jax.sharding import PartitionSpec as P

BLOCK = 64
HIGH_ACCURACY = lax.Precision.HIGHEST


def as_sent(array):

    def short(part):
        return part.astype(jnp.bfloat16) if part.dtype == jnp.float32 else part

    return jax.tree.map(short, array)


def passed_along(array, axis, by):
    count = lax.axis_size(axis)
    pairs = [(i, i + by) for i in range(count) if 0 <= i + by < count]
    return lax.ppermute(array, axis, pairs)


def entering(value, axis, join, neutral):
    count, mine = (lax.axis_size(axis), lax.axis_index(axis))
    pieces = jax.tree.map(lambda part: lax.all_gather(part, axis), value)
    subtotal = jax.tree.map(
        lambda part, zero: jnp.full_like(part, 0) + jnp.asarray(zero, part.dtype), value, neutral
    )

    def hop(position, subtotal):
        longer = join(subtotal, jax.tree.map(lambda part: part[position], pieces))
        return jax.tree.map(lambda new, old: jnp.where(position < mine, new, old), longer, subtotal)

    return lax.fori_loop(0, count - 1, hop, subtotal)


def norm_rows(matrix, norm_gain):
    values = matrix.astype(jnp.float32)
    center = values - jnp.mean(values, axis=-1, keepdims=True)
    spread = jnp.mean(center * center, axis=-1, keepdims=True)
    return (center * lax.rsqrt(spread + 1e-05) * norm_gain).astype(jnp.bfloat16)


def block_chain(query, keys, values, decay):
    heads, length, width = query.shape
    count = length // BLOCK

    def split_blocks(array):
        return array.reshape(heads, count, BLOCK, array.shape[-1]).transpose(1, 0, 2, 3)

    causal = jnp.tril(jnp.ones((BLOCK, BLOCK), jnp.float32))

    def advance(hidden_state, inputs):
        query_part, key_portion, value_portion, decay_part = inputs
        running_state = jnp.cumsum(decay_part, axis=1)
        scaled_query = query_part * jnp.exp(running_state)
        key_scaled = key_portion * jnp.exp(-running_state)
        scores = (
            jnp.einsum("htk,hsk->hts", scaled_query, key_scaled, precision=HIGH_ACCURACY) * causal
        )
        inside = jnp.einsum("hts,hsv->htv", scores, value_portion, precision=HIGH_ACCURACY)
        carried_state = jnp.einsum(
            "rgn,rns->rgs", scaled_query, hidden_state, precision=HIGH_ACCURACY
        )
        final_state = running_state[:, -1:, :]
        state_update = jnp.einsum(
            "qdm,qdt->qmt",
            key_portion * jnp.exp(final_state - running_state),
            value_portion,
            precision=HIGH_ACCURACY,
        )
        return (
            jnp.exp(final_state[:, 0, :])[:, :, None] * hidden_state + state_update,
            inside + carried_state,
        )

    initial = jnp.zeros((heads, width, values.shape[-1]), jnp.float32)
    hidden_state, layer_results = lax.scan(
        advance,
        initial,
        (split_blocks(query), split_blocks(keys), split_blocks(values), split_blocks(decay)),
    )
    return (
        layer_results.transpose(1, 0, 2, 3).reshape(heads, length, values.shape[-1]),
        hidden_state,
    )


def chain_join(earlier_tokens, later):
    return (
        earlier_tokens[0] + later[0],
        jnp.exp(later[0])[:, :, None] * earlier_tokens[1] + later[1],
    )


def body(
    tokens,
    norm_gain,
    conv_gate_w,
    conv_in_w,
    query_w,
    forget_w,
    value_w,
    conv_taps,
    floor_gate,
    leak,
    head_gain,
    conv_out_w,
    chain_out_w,
):
    own_rows = norm_rows(tokens[0], norm_gain)
    normed = lax.all_gather(own_rows, "tp", axis=0, tiled=True)
    length = normed.shape[0]
    weights = (conv_gate_w, conv_in_w, query_w, forget_w, value_w)
    groups = lax.axis_size("fs")
    member = lax.axis_index("fs")
    sliced = tuple(
        (
            lax.dynamic_slice_in_dim(
                weight, member * (weight.shape[1] // groups), weight.shape[1] // groups, 1
            )
            for weight in weights
        )
    )
    pooled = lax.all_gather(normed[None], "fs", axis=0, tiled=True)
    flat_rows = pooled.reshape(groups * length, pooled.shape[2])
    pieces = jax.tree.map(
        lambda part: lax.all_gather(part, "sp", axis=0, tiled=True), as_sent(sliced)
    )
    sums = tuple(
        (jnp.dot(flat_rows, piece, preferred_element_type=jnp.float32) for piece in pieces)
    )
    quarters = tuple(
        (total.astype(jnp.bfloat16).reshape(groups, length, total.shape[1]) for total in sums)
    )
    returned = jax.tree.map(
        lambda part, own: part.astype(own.dtype),
        lax.all_to_all(as_sent(quarters), "fs", split_axis=0, concat_axis=2, tiled=True),
        quarters,
    )
    projected = tuple((column_set[0] for column_set in returned))
    second_gate, signal, query_raw, forget_raw, value_raw = projected
    margin = conv_taps.shape[0] - 1
    rim = passed_along(signal[length - margin :], "sp", 1)
    padded = jnp.concatenate([rim, signal], axis=0).astype(jnp.float32)
    filtered = jnp.zeros((length, signal.shape[1]), jnp.float32)
    for offset in range(margin + 1):
        filtered = filtered + conv_taps[offset] * padded[offset : offset + length]
    conv_mix = (second_gate.astype(jnp.float32) * filtered).astype(jnp.bfloat16)
    heads_here = leak.shape[2]
    head_width = query_raw.shape[1] // heads_here

    def by_head(array):
        return array.astype(jnp.float32).reshape(length, heads_here, head_width).transpose(1, 0, 2)

    floor = floor_gate.reshape(heads_here, 1, head_width)
    logits = by_head(forget_raw)
    retain = floor + (1.0 - floor) * jax.nn.sigmoid(logits)
    keys = (1.0 - floor) * jax.nn.sigmoid(-logits)
    decay = jnp.log(retain) + leak[0].T[:, :, None]
    query = jax.nn.silu(by_head(query_raw))
    pairwise_dot, hidden_state = block_chain(query, keys, by_head(value_raw), decay)
    total_decay = jnp.sum(decay, axis=1)
    identity = (jnp.zeros_like(total_decay), jnp.zeros_like(hidden_state))
    earlier_tokens = entering((total_decay, hidden_state), "sp", chain_join, identity)
    filter_reach = query * jnp.exp(jnp.cumsum(decay, axis=1))
    recurrence_raw = pairwise_dot + jnp.einsum(
        "rgn,rns->rgs", filter_reach, earlier_tokens[1], precision=HIGH_ACCURACY
    )
    scale = lax.rsqrt(jnp.mean(recurrence_raw * recurrence_raw, axis=-1, keepdims=True) + 1e-06)
    chain_mix = (
        (recurrence_raw * scale * head_gain)
        .transpose(1, 0, 2)
        .reshape(length, heads_here * head_width)
        .astype(jnp.bfloat16)
    )
    conv_full, chain_full = (
        lax.all_gather(conv_out_w, "fs", axis=1, tiled=True),
        lax.all_gather(chain_out_w, "fs", axis=1, tiled=True),
    )
    mixed = lax.psum_scatter(
        jnp.dot(conv_mix, conv_full, preferred_element_type=jnp.float32)
        + jnp.dot(chain_mix, chain_full, preferred_element_type=jnp.float32),
        "tp",
        scatter_dimension=0,
        tiled=True,
    )
    return mixed.astype(jnp.bfloat16)[None]


def solution(mesh):
    in_specs = (
        P("fs", ("sp", "tp"), None),
        P(),
        P("sp", "tp"),
        P("sp", "tp"),
        P("sp", "tp"),
        P("sp", "tp"),
        P("sp", "tp"),
        P(None, "tp"),
        P("tp"),
        P("fs", "sp", "tp"),
        P(),
        P("tp", "fs"),
        P("tp", "fs"),
    )
    out_specs = P("fs", ("sp", "tp"), None)
    return jax.shard_map(body, mesh=mesh, in_specs=in_specs, out_specs=out_specs, check_vma=False)
```

profile of v0, /device:TPU:0, one launch (start us, length us, event | category | flops | bytes accessed | tf_op | source)
XLA Modules:
  0.0 289.1 jit_solution(1176081124464315372)
XLA Ops:
  6.5 1.4 convert_reduce_fusion
  8.0 1.5 fusion.29
  9.5 2.0 fusion.31
  11.6 12.6 %all-gather.10.cloned.1.call-done = bf16[384,2048]{1,0:T(8,128)(2,1)} async-done(((bf16[192,2048]{1,0:T(8,128)(2,1)}), bf16[384,2048]{1,0:T(8,128)(2,1)}) %all-gather.10.cloned.1.call-update) | async-done | bytes 1572880 | tf_op jit(solution)/shard_map/all_gather | solution.py:113
  24.3 0.7 all-gather.12.cloned.1.call-update
  25.0 16.3 %all_gather.44 = bf16[2048,128]{1,0:T(8,128)(2,1)S(1)} all-gather(bf16[512,128]{1,0:T(8,128)(2,1)S(1)} %constant_dynamic-slice_fusion.2), channel_id=1, replica_groups=mesh['sp'=4,'fs'=4,'tp'=2] {'sp'}, dimensions={0}, use_global_device_ids=true | all-gather | bytes 655360 | tf_op jit(solution)/shard_map/all_gather | solution.py:129
  41.4 0.9 constant_dynamic-slice_fusion
  42.3 16.1 %all_gather.46 = bf16[2048,128]{1,0:T(8,128)(2,1)S(1)} all-gather(bf16[512,128]{1,0:T(8,128)(2,1)S(1)} %constant_dynamic-slice_fusion), channel_id=1, replica_groups=mesh['sp'=4,'fs'=4,'tp'=2] {'sp'}, dimensions={0}, use_global_device_ids=true | all-gather | bytes 655360 | tf_op jit(solution)/shard_map/all_gather | solution.py:129
  58.4 0.9 constant_dynamic-slice_fusion.1
  59.3 15.8 %all_gather.45 = bf16[2048,128]{1,0:T(8,128)(2,1)S(1)} all-gather(bf16[512,128]{1,0:T(8,128)(2,1)S(1)} %constant_dynamic-slice_fusion.1), channel_id=1, replica_groups=mesh['sp'=4,'fs'=4,'tp'=2] {'sp'}, dimensions={0}, use_global_device_ids=true | all-gather | bytes 655360 | tf_op jit(solution)/shard_map/all_gather | solution.py:129
  75.1 22.2 %all-gather.16.cloned.1.call-done = bf16[1536,2048]{1,0:T(8,128)(2,1)} async-done(((bf16[384,2048]{1,0:T(8,128)(2,1)}), bf16[1536,2048]{1,0:T(8,128)(2,1)}) %all-gather.16.cloned.1.call-update) | async-done | bytes 6291472 | tf_op jit(solution)/shard_map/all_gather | solution.py:126
  97.3 5.4 %convolution_convert_fusion.2 = bf16[1536,128]{1,0:T(8,128)(2,1)} fusion(bf16[1536,2048]{1,0:T(8,128)(2,1)} %all-gather.16.cloned.1.call-done, bf16[2048,128]{1,0:T(8,128)(2,1)S(1)} %all_gather.44), kind=kOutput, calls=%fused_computation.38 | convolution fusion | flops 805502976 | bytes 7208960 | tf_op jit(solution)/shard_map/dot_general | solution.py:132
  102.6 3.5 %all-to-all-start.2 = ((bf16[4,384,128]{2,1,0:T(8,128)(2,1)}), bf16[4,384,128]{2,1,0:T(8,128)(2,1)S(1)}, u32[]{:S(2)}, u32[]{:S(2)}) async-start(bf16[4,384,128]{2,1,0:T(8,128)(2,1)} %bitcast.15), calls=%async_computation.2 | async-start | bytes 786432 | tf_op jit(solution)/shard_map/all_to_all | solution.py:139
  106.1 5.7 %convolution_convert_fusion = bf16[1536,128]{1,0:T(8,128)(2,1)} fusion(bf16[1536,2048]{1,0:T(8,128)(2,1)} %all-gather.16.cloned.1.call-done, bf16[2048,128]{1,0:T(8,128)(2,1)S(1)} %all_gather.46), kind=kOutput, calls=%fused_computation.36 | convolution fusion | flops 805502976 | bytes 7208960 | tf_op jit(solution)/shard_map/dot_general | solution.py:132
  111.8 2.6 convolution_convert_fusion.1
  114.4 2.7 all-to-all-done.2
  117.1 3.5 %all-to-all-start.3 = ((bf16[4,384,128]{2,1,0:T(8,128)(2,1)}), bf16[4,384,128]{2,1,0:T(8,128)(2,1)S(1)}, u32[]{:S(2)}, u32[]{:S(2)}) async-start(bf16[4,384,128]{2,1,0:T(8,128)(2,1)} %bitcast.30), calls=%async_computation.3 | async-start | bytes 786432 | tf_op jit(solution)/shard_map/all_to_all | solution.py:139
  121.7 0.8 copy-done.3
  122.5 2.6 add_exponential_fusion
  125.0 2.2 all-to-all-done.3
  127.2 3.5 %all-to-all-start.4 = ((bf16[4,384,128]{2,1,0:T(8,128)(2,1)}), bf16[4,384,128]{2,1,0:T(8,128)(2,1)S(1)}, u32[]{:S(2)}, u32[]{:S(2)}) async-start(bf16[4,384,128]{2,1,0:T(8,128)(2,1)} %bitcast.33), calls=%async_computation.4 | async-start | bytes 786432 | tf_op jit(solution)/shard_map/all_to_all | solution.py:139
  130.8 2.2 copy.35
  133.0 1.9 fusion.52
  134.8 6.2 %all-to-all-done.4 = bf16[4,384,128]{2,1,0:T(8,128)(2,1)S(1)} async-done(((bf16[4,384,128]{2,1,0:T(8,128)(2,1)}), bf16[4,384,128]{2,1,0:T(8,128)(2,1)S(1)}, u32[]{:S(2)}, u32[]{:S(2)}) %all-to-all-start.4) | async-done | bytes 393248 | tf_op jit(solution)/shard_map/all_to_all | solution.py:139
  141.1 2.2 bitcast_multiply_fusion.7
  143.3 20.6 %while.27 = (s32[]{:T(128)}, f32[4,128,128]{2,1,0:T(8,128)S(1)}, f32[6,4,64,128]{3,2,0,1:T(8,128)}, f32[6,4,64,128]{3,2,0,1:T(8,128)}, f32[6,4,64,128]{3,2,0,1:T...) while((s32[]{:T(128)}, f32[4,128,128]{2,1,0:T(8,128)S(1)}, ...), condition=%wide.region_4.5_spmd.clone, body=%wide.region_2.4_spmd.clone.sunk | while | flops 153575424 | bytes 3275900 | solution.py:79
  143.3 0.9 dynamic-slice_bitcast_fusion.2
  145.0 1.0 fusion.86
  146.7 0.9 dynamic-slice_bitcast_fusion.2
  148.4 1.0 fusion.86
  150.2 0.9 dynamic-slice_bitcast_fusion.2
  151.9 1.0 fusion.86
  153.6 0.9 dynamic-slice_bitcast_fusion.2
  155.3 1.0 fusion.86
  157.0 0.9 dynamic-slice_bitcast_fusion.2
  158.7 1.0 fusion.86
  160.5 0.9 dynamic-slice_bitcast_fusion.2
  162.2 1.0 fusion.86
  163.2 0.7 convolution_add_fusion.5
  163.9 0.7 copy-done.1
  164.6 0.9 constant_dynamic-slice_fusion.3
  165.6 0.9 constant_dynamic-slice_fusion.4
  166.5 21.4 %all_gather.42 = bf16[2048,128]{1,0:T(8,128)(2,1)S(1)} all-gather(bf16[512,128]{1,0:T(8,128)(2,1)S(1)} %constant_dynamic-slice_fusion.3), channel_id=1, replica_groups=mesh['sp'=4,'fs'=4,'tp'=2] {'sp'}, dimensions={0}, use_global_device_ids=true | all-gather | bytes 655360 | tf_op jit(solution)/shard_map/all_gather | solution.py:129
  187.9 18.9 %all_gather.41 = bf16[2048,128]{1,0:T(8,128)(2,1)S(1)} all-gather(bf16[512,128]{1,0:T(8,128)(2,1)S(1)} %constant_dynamic-slice_fusion.4), channel_id=1, replica_groups=mesh['sp'=4,'fs'=4,'tp'=2] {'sp'}, dimensions={0}, use_global_device_ids=true | all-gather | bytes 655360 | tf_op jit(solution)/shard_map/all_gather | solution.py:129
  206.9 4.6 %convolution_convert_fusion.3 = bf16[1536,128]{1,0:T(8,128)(2,1)S(1)} fusion(bf16[1536,2048]{1,0:T(8,128)(2,1)} %all-gather.16.cloned.1.call-done, bf16[2048,128]{1,0:T(8,128)(2,1)S(1)} %all_gather.42), kind=kOutput, calls=%fused_computation.39 | convolution fusion | flops 805502976 | bytes 7208960 | tf_op jit(solution)/shard_map/dot_general | solution.py:132
  211.4 1.0 copy.28
  212.4 3.5 %all-to-all-start.1 = ((bf16[4,384,128]{1,2,0:T(8,128)(2,1)}), bf16[4,384,128]{1,2,0:T(8,128)(2,1)S(1)}, u32[]{:S(2)}, u32[]{:S(2)}) async-start(bf16[4,384,128]{1,2,0:T(8,128)(2,1)} %copy.28), calls=%async_computation.1 | async-start | bytes 786432 | tf_op jit(solution)/shard_map/all_to_all | solution.py:139
  215.9 4.6 %convolution_convert_fusion.4 = bf16[1536,128]{1,0:T(8,128)(2,1)S(1)} fusion(bf16[1536,2048]{1,0:T(8,128)(2,1)} %all-gather.16.cloned.1.call-done, bf16[2048,128]{1,0:T(8,128)(2,1)S(1)} %all_gather.41), kind=kOutput, calls=%fused_computation.40 | convolution fusion | flops 805502976 | bytes 7208960 | tf_op jit(solution)/shard_map/dot_general | solution.py:132
  220.5 0.9 copy.27
  221.7 3.9 %all-to-all-start = ((bf16[4,384,128]{1,2,0:T(8,128)(2,1)}), bf16[4,384,128]{1,2,0:T(8,128)(2,1)S(1)}, u32[]{:S(2)}, u32[]{:S(2)}) async-start(bf16[4,384,128]{1,2,0:T(8,128)(2,1)} %copy.27), calls=%async_computation | async-start | bytes 786432 | tf_op jit(solution)/shard_map/all_to_all | solution.py:139
  226.6 2.2 collective-permute-start
  228.9 2.6 all-to-all-done
  231.5 11.9 %all-gather.3 = f32[4,4,128]{2,1,0:T(4,128)S(1)} all-gather(f32[1,4,128]{2,1,0:T(4,128)S(1)} %bitcast.201), channel_id=3, replica_groups=mesh['sp'=4,'fs'=4,'tp'=2] {'sp'}, dimensions={0}, use_global_device_ids=true | all-gather | bytes 10240 | tf_op jit(solution)/shard_map/all_gather | solution.py:26
  243.8 0.7 fusion.50
  244.5 4.2 %fusion.54 = f32[384,2048]{1,0:T(8,128)} fusion(bf16[384,512]{0,1:T(8,128)(2,1)S(1)} %fusion.50, bf16[512,2048]{1,0:T(8,128)(2,1)} %all-gather.12.cloned.1.call-done), kind=kOutput, calls=%fused_computation.99 | convolution fusion | flops 805306368 | bytes 5636096 | tf_op jit(solution)/shard_map/dot_general | solution.py:183
  248.8 3.7 %while.28 = (s32[]{:T(128)}, f32[4,128,128]{2,1,0:T(8,128)S(1)}, s32[]{:T(128)}, f32[4,4,128]{2,1,0:T(4,128)S(1)}, f32[4,4,128,128]{3,2,1,0:T(8,128)}, /*index=5*/s32[]{:T(128)}, s32[]{:T(128)}) while((s32[]{:T(128)}, f32[4,128,128]{2,1,0:T(8,128)S(1)}, s32[]{:T(128)}, f32[4,4,128]{2,1,0:T(4,128)S(1)}, ...), condition=%wide.region_9.10_spmd.clone, body=%wide.region_8.9_spmd.clone.sunk | while | flops 262148 | bytes 792681 | solution.py:35
  248.8 1.2 fusion.87
  250.1 1.2 fusion.87
  251.3 1.2 fusion.87
  252.5 1.1 multiply_reduce_fusion
  253.8 9.6 %all-gather.14.cloned.1.call-done = bf16[512,2048]{1,0:T(8,128)(2,1)} async-done(((bf16[512,512]{1,0:T(8,128)(2,1)}), bf16[512,2048]{1,0:T(8,128)(2,1)}) %all-gather.14.cloned.1.call-update) | async-done | bytes 2097168 | tf_op jit(solution)/shard_map/all_gather | solution.py:180
  263.3 5.2 %convolution_add_fusion.2 = f32[384,2048]{1,0:T(8,128)} fusion(f32[384,2048]{1,0:T(8,128)} %fusion.54, bf16[384,512]{0,1:T(8,128)(2,1)S(1)} %bitcast.187, bf16[512,2048]{1,0:T(8,128)(2,1)} %all-gather.14.cloned.1.call-done), kind=kOutput, calls=%fused_computation.35 | convolution fusion | flops 806092800 | bytes 8781824 | tf_op jit(solution)/shard_map/dot_general | solution.py:184
  268.5 11.3 %reduce-scatter.2.cloned.1.call-done = f32[192,2048]{1,0:T(8,128)} async-done(((f32[384,2048]{1,0:T(8,128)}), f32[192,2048]{1,0:T(8,128)}) %reduce-scatter.2.cloned.1.call-update) | async-done | bytes 1572880 | tf_op jit(solution)/shard_map/reduce_scatter | solution.py:182
  279.9 2.4 convert_bitcast_fusion.2
  (101 shorter events, 11.2 us)
Async XLA Ops:
  6.5 18.4 %copy-start = (bf16[512,512]{1,0:T(8,128)(2,1)S(1)}, bf16[512,512]{1,0:T(8,128)(2,1)}, u32[]{:S(2)}) copy-start(bf16[512,512]{1,0:T(8,128)(2,1)} %param.22) | copy-start | bytes 1572868
  6.5 2.9 %copy-start.2 = (bf16[1,192,2048]{2,1,0:T(8,128)(2,1)S(1)}, bf16[1,192,2048]{2,1,0:T(8,128)(2,1)}, u32[]{:S(2)}) copy-start(bf16[1,192,2048]{2,1,0:T(8,128)(2,1)} %param.17) | copy-start | bytes 2359300
  6.5 17.7 %all-gather.10.cloned.1.call-start = ((), (), s32[]{:S(2)}) async-start(), calls=%async_computation.6 | async-start | bytes 2359296 | tf_op jit(solution)/shard_map/all_gather | solution.py:113
  11.5 29.9 %copy-start.7 = (f32[512]{0:T(512)S(1)}, f32[512]{0:T(512)}, u32[]{:S(2)}) copy-start(f32[512]{0:T(512)} %param.25) | copy-start | bytes 6148
  11.5 85.8 %all-gather.16.cloned.1.call-start = ((), (), s32[]{:S(2)}) async-start(), calls=%async_computation.10 | async-start | bytes 7864320 | tf_op jit(solution)/shard_map/all_gather | solution.py:126
  24.2 220.3 %all-gather.12.cloned.1.call-start = ((), (), s32[]{:S(2)}) async-start(), calls=%async_computation.7 | async-start | bytes 2621440 | tf_op jit(solution)/shard_map/all_gather | solution.py:179
  102.6 14.4 %all-to-all-start.2 = ((bf16[4,384,128]{2,1,0:T(8,128)(2,1)}), bf16[4,384,128]{2,1,0:T(8,128)(2,1)S(1)}, u32[]{:S(2)}, u32[]{:S(2)}) async-start(bf16[4,384,128]{2,1,0:T(8,128)(2,1)} %bitcast.15), calls=%async_computation.2 | async-start | bytes 786432 | tf_op jit(solution)/shard_map/all_to_all | solution.py:139
  106.1 5.7 %copy-start.11 = (bf16[1536,2048]{1,0:T(8,128)(2,1)S(1)}, bf16[1536,2048]{1,0:T(8,128)(2,1)}, u32[]{:S(2)}) copy-start(bf16[1536,2048]{1,0:T(8,128)(2,1)} %all-gather.16.cloned.1.call-done) | copy-start | bytes 18874372
  111.8 8.7 %copy-start.6 = (f32[1,384,4]{1,2,0:T(4,128)S(1)}, f32[1,384,4]{1,2,0:T(4,128)}, u32[]{:S(2)}) copy-start(f32[1,384,4]{1,2,0:T(4,128)} %param.26) | copy-start | bytes 18436
  117.1 10.1 %all-to-all-start.3 = ((bf16[4,384,128]{2,1,0:T(8,128)(2,1)}), bf16[4,384,128]{2,1,0:T(8,128)(2,1)S(1)}, u32[]{:S(2)}, u32[]{:S(2)}) async-start(bf16[4,384,128]{2,1,0:T(8,128)(2,1)} %bitcast.30), calls=%async_computation.3 | async-start | bytes 786432 | tf_op jit(solution)/shard_map/all_to_all | solution.py:139
  121.4 1.0 copy-start.3
  127.2 13.9 %all-to-all-start.4 = ((bf16[4,384,128]{2,1,0:T(8,128)(2,1)}), bf16[4,384,128]{2,1,0:T(8,128)(2,1)S(1)}, u32[]{:S(2)}, u32[]{:S(2)}) async-start(bf16[4,384,128]{2,1,0:T(8,128)(2,1)} %bitcast.33), calls=%async_computation.4 | async-start | bytes 786432 | tf_op jit(solution)/shard_map/all_to_all | solution.py:139
  130.7 118.1 %all-gather.18.cloned.1.call-start = ((), (), s32[]{:S(2)}) async-start(), calls=%async_computation.11 | async-start | bytes 1310720 | tf_op jit(solution)/shard_map/all_gather | solution.py:26
  163.9 0.7 copy-start.1
  212.4 9.3 %all-to-all-start.1 = ((bf16[4,384,128]{1,2,0:T(8,128)(2,1)}), bf16[4,384,128]{1,2,0:T(8,128)(2,1)S(1)}, u32[]{:S(2)}, u32[]{:S(2)}) async-start(bf16[4,384,128]{1,2,0:T(8,128)(2,1)} %copy.28), calls=%async_computation.1 | async-start | bytes 786432 | tf_op jit(solution)/shard_map/all_to_all | solution.py:139
  220.4 5.8 %copy-start.9 = (f32[3,512]{1,0:T(4,128)S(1)}, f32[3,512]{1,0:T(4,128)}, u32[]{:S(2)}) copy-start(f32[3,512]{1,0:T(4,128)} %param.24) | copy-start | bytes 18436
  220.5 5.8 %copy-start.5 = (f32[6,4,64,128]{3,2,0,1:T(8,128)S(1)}, f32[6,4,64,128]{3,2,0,1:T(8,128)}, u32[]{:S(2)}) copy-start(f32[6,4,64,128]{3,2,0,1:T(8,128)} %get-tuple-element.142) | copy-start | bytes 2359300
  221.4 10.1 %copy-start.8 = (f32[4,128]{1,0:T(4,128)S(1)}, f32[4,128]{1,0:T(4,128)}, u32[]{:S(2)}) copy-start(f32[4,128]{1,0:T(4,128)} %get-tuple-element.227) | copy-start | bytes 6148
  221.7 9.7 %all-to-all-start = ((bf16[4,384,128]{1,2,0:T(8,128)(2,1)}), bf16[4,384,128]{1,2,0:T(8,128)(2,1)S(1)}, u32[]{:S(2)}, u32[]{:S(2)}) async-start(bf16[4,384,128]{1,2,0:T(8,128)(2,1)} %copy.27), calls=%async_computation | async-start | bytes 786432 | tf_op jit(solution)/shard_map/all_to_all | solution.py:139
  225.6 37.8 %all-gather.14.cloned.1.call-start = ((), (), s32[]{:S(2)}) async-start(), calls=%async_computation.8 | async-start | bytes 2621440 | tf_op jit(solution)/shard_map/all_gather | solution.py:180
  226.1 53.7 %reduce-scatter.2.cloned.1.call-start = ((), (), s32[]{:S(2)}) async-start(), calls=%async_computation.9 | async-start | bytes 4718592 | tf_op jit(solution)/shard_map/reduce_scatter | solution.py:182
  226.6 16.8 %collective-permute-start = (bf16[2,512]{0,1:T(8,128)(2,1)S(1)}, bf16[2,512]{0,1:T(8,128)(2,1)S(1)}, u32[]{:S(2)}, u32[]{:S(2)}) collective-permute-start(bf16[2,512]{0,1:T(8,128)(2,1)S(1)} %bitcast.195), channel_id=1, source_target_pairs={{0,8},{8,16},{16,24},{1,9},{9,17},{17,25},{2,10},{10,18},{18,26},{... | collective-permute-start | bytes 6152 | tf_op jit(solution)/shard_map/ppermute | solution.py:21
  248.8 3.7 %copy-start.4 = (f32[4,384,128]{2,1,0:T(8,128)S(1)}, f32[4,384,128]{2,1,0:T(8,128)}, u32[]{:S(2)}) copy-start(f32[4,384,128]{2,1,0:T(8,128)} %get-tuple-element.229) | copy-start | bytes 2359300
  252.4 1.2 copy-start.10
Sparse Core Ops, SparseCore 0:
  11.6 12.5 all-gather.9
  26.0 71.1 all-gather.15
  99.1 42.9 all-gather.11
  164.8 37.6 all-gather.17
  227.9 35.3 all-gather.13
  268.6 11.1 reduce-scatter.1
where the time goes:
time: 290 us; the launch traced here: 289 us
  blocking collectives  101 us (35%)
  waiting for transfers between devices  71 us (24%)
  matrix products  47.2 us (16%)
  other arithmetic  20.8 us (7%)
  starting transfers between devices  20.1 us (7%)
  local copies, waits for them, and re-layouts  15.3 us (5%)
  between operations  13.8 us (5%)
    all_gather x5, blocking collectives, body(): lax.all_gather(part, 'sp', axis=0, tiled=True)  88.6 us
    dot_general x5, matrix products, body(): jnp.dot(flat_rows, piece, preferred_element_type=jnp.float32)  22.8 us
    all_gather x1, waiting for transfers between devices, body(): pooled = lax.all_gather(normed[None], 'fs', axis=0, tiled=True)  22.2 us
    all_to_all x5, starting transfers between devices, body(): lax.all_to_all(as_sent(quarters), 'fs', split_axis=0, concat_axis=2, tile...  17.7 us
    all_to_all x5, waiting for transfers between devices, body(): lax.all_to_all(as_sent(quarters), 'fs', split_axis=0, concat_axis=2, tile...  14 us
    all_gather x1, waiting for transfers between devices, body(): normed = lax.all_gather(own_rows, 'tp', axis=0, tiled=True)  12.6 us
    all_gather x1, blocking collectives, entering(): pieces = jax.tree.map(lambda part: lax.all_gather(part, axis), value)  11.9 us
    reduce_scatter x1, waiting for transfers between devices, body(): lax.psum_scatter(jnp.dot(conv_mix, conv_full, preferred_element_type=jnp....  11.3 us
  transfers between devices with their start and end apart: 12, of which 9 were waited for; matrix products, arithmetic and copies ran while one was open for 24% of the time, Pallas kernels for 0%

commit v1 on v0

--- a/solution.py
+++ b/solution.py
@@ -123,7 +123,9 @@
             for weight in weights
         )
     )
-    pooled = lax.all_gather(normed[None], "fs", axis=0, tiled=True)
+    pooled = jnp.concatenate(
+        lax.all_to_all(jnp.stack([normed[None]] * lax.axis_size("fs")), "fs", 0, 0), axis=0
+    )
     flat_rows = pooled.reshape(groups * length, pooled.shape[2])
     pieces = jax.tree.map(
         lambda part: lax.all_gather(part, "sp", axis=0, tiled=True), as_sent(sliced)

time: 290 us -> 311 us (1.072)
  waiting for transfers between devices: 71 us -> 77.2 us
  starting transfers between devices: 20.1 us -> 25.2 us
  local copies, waits for them, and re-layouts: 15.3 us -> 20.3 us
    all_to_all x0 -> x1, waiting for transfers between devices: none -> 36.7 us  [body(): lax.all_to_all(jnp.stack([normed[None]] * lax.axis_size('fs')), 'fs', 0, 0)]
    all_gather x1 -> x0, waiting for transfers between devices: 22.2 us -> none  [body(): pooled = lax.all_gather(normed[None], 'fs', axis=0, tiled=True)]
    all_to_all x5, waiting for transfers between devices: 14 us -> 6.77 us  [body(): lax.all_to_all(as_sent(quarters), 'fs', split_axis=0, concat_axis=2, tile...]
    all_to_all x0 -> x1, starting transfers between devices: none -> 5.26 us  [body(): lax.all_to_all(jnp.stack([normed[None]] * lax.axis_size('fs')), 'fs', 0, 0)]
    another operation x1 -> x2, local copies, waits for them, and re-layouts: 0.01 us -> 4.84 us  [the longest x1 4.83 us: body(): jnp.stack([normed[None]] * lax.axis_size('fs'))]
  transfers between devices with their start and end apart: 12 -> 12, of which waited for: 9 -> 8; matrix products, arithmetic and copies ran while one was open for 24% -> 23% of each run, Pallas kernels for 0% -> 0%
where the time goes in v1:
time: 311 us; the launch traced here: 310 us
  blocking collectives  101 us (32%)
  waiting for transfers between devices  77.2 us (25%)
  matrix products  49.8 us (16%)
  starting transfers between devices  25.2 us (8%)
  other arithmetic  21.1 us (7%)
  local copies, waits for them, and re-layouts  20.3 us (7%)
  between operations  15.3 us (5%)
    all_gather x5, blocking collectives, body(): lax.all_gather(part, 'sp', axis=0, tiled=True)  88.6 us
    all_to_all x1, waiting for transfers between devices, body(): lax.all_to_all(jnp.stack([normed[None]] * lax.axis_size('fs')), 'fs', 0, 0)  36.7 us
    dot_general x5, matrix products, body(): jnp.dot(flat_rows, piece, preferred_element_type=jnp.float32)  25.3 us
    all_to_all x5, starting transfers between devices, body(): lax.all_to_all(as_sent(quarters), 'fs', split_axis=0, concat_axis=2, tile...  18.5 us
    all_gather x1, waiting for transfers between devices, body(): normed = lax.all_gather(own_rows, 'tp', axis=0, tiled=True)  12.7 us
    all_gather x1, blocking collectives, entering(): pieces = jax.tree.map(lambda part: lax.all_gather(part, axis), value)  11.9 us
    reduce_scatter x1, waiting for transfers between devices, body(): lax.psum_scatter(jnp.dot(conv_mix, conv_full, preferred_element_type=jnp....  11.3 us
    all_gather x1, waiting for transfers between devices, body(): lax.all_gather(chain_out_w, 'fs', axis=1, tiled=True)  8.58 us
  transfers between devices with their start and end apart: 12, of which 8 were waited for; matrix products, arithmetic and copies ran while one was open for 23% of the time, Pallas kernels for 0%

profile of v1, /device:TPU:0, one launch (start us, length us, event | category | flops | bytes accessed | tf_op | source)
XLA Modules:
  0.0 309.9 jit_solution(3195687829998906094)
XLA Ops:
  7.4 1.4 convert_reduce_fusion
  8.8 1.5 fusion.29
  10.2 2.5 fusion.31
  12.7 12.7 %all-gather.8.cloned.1.call-done = bf16[384,2048]{1,0:T(8,128)(2,1)} async-done(((bf16[192,2048]{1,0:T(8,128)(2,1)}), bf16[384,2048]{1,0:T(8,128)(2,1)}) %all-gather.8.cloned.1.call-update) | async-done | bytes 1572880 | tf_op jit(solution)/shard_map/all_gather | solution.py:113
  25.4 4.8 %stack.3 = bf16[4,1,384,2048]{3,2,1,0:T(8,128)(2,1)} broadcast(bf16[384,2048]{1,0:T(8,128)(2,1)} %all-gather.8.cloned.1.call-done), dimensions={2,3} | broadcast | bytes 7864320 | tf_op jit(solution)/shard_map/stack | solution.py:127
  30.2 5.3 %all-to-all-start = ((bf16[4,1,384,2048]{3,2,1,0:T(8,128)(2,1)}), bf16[4,1,384,2048]{3,2,1,0:T(8,128)(2,1)}, u32[]{:S(2)}, u32[]{:S(2)}) async-start(bf16[4,1,384,2048]{3,2,1,0:T(8,128)(2,1)} %stack.3), calls=%async_computation | async-start | bytes 12582912 | tf_op jit(solution)/shard_map/all_to_all | solution.py:127
  36.2 0.9 constant_dynamic-slice_fusion
  37.1 0.9 constant_dynamic-slice_fusion.1
  38.0 16.3 %all_gather.40 = bf16[2048,128]{1,0:T(8,128)(2,1)S(1)} all-gather(bf16[512,128]{1,0:T(8,128)(2,1)S(1)} %constant_dynamic-slice_fusion.2), channel_id=1, replica_groups=mesh['sp'=4,'fs'=4,'tp'=2] {'sp'}, dimensions={0}, use_global_device_ids=true | all-gather | bytes 655360 | tf_op jit(solution)/shard_map/all_gather | solution.py:131
  54.3 16.1 %all_gather.42 = bf16[2048,128]{1,0:T(8,128)(2,1)S(1)} all-gather(bf16[512,128]{1,0:T(8,128)(2,1)S(1)} %constant_dynamic-slice_fusion), channel_id=1, replica_groups=mesh['sp'=4,'fs'=4,'tp'=2] {'sp'}, dimensions={0}, use_global_device_ids=true | all-gather | bytes 655360 | tf_op jit(solution)/shard_map/all_gather | solution.py:131
  70.3 15.9 %all_gather.41 = bf16[2048,128]{1,0:T(8,128)(2,1)S(1)} all-gather(bf16[512,128]{1,0:T(8,128)(2,1)S(1)} %constant_dynamic-slice_fusion.1), channel_id=1, replica_groups=mesh['sp'=4,'fs'=4,'tp'=2] {'sp'}, dimensions={0}, use_global_device_ids=true | all-gather | bytes 655360 | tf_op jit(solution)/shard_map/all_gather | solution.py:131
  86.2 36.7 %all-to-all-done = bf16[4,1,384,2048]{3,2,1,0:T(8,128)(2,1)} async-done(((bf16[4,1,384,2048]{3,2,1,0:T(8,128)(2,1)}), bf16[4,1,384,2048]{3,2,1,0:T(8,128)(2,1)}, u32[]{:S(2)}, u32[]{:S(2)}) %all-to-all-start) | async-done | bytes 6291488 | tf_op jit(solution)/shard_map/all_to_all | solution.py:127
  122.9 5.3 %convolution_convert_fusion.2 = bf16[1536,128]{1,0:T(8,128)(2,1)} fusion(bf16[1536,2048]{1,0:T(8,128)(2,1)} %bitcast.1, bf16[2048,128]{1,0:T(8,128)(2,1)S(1)} %all_gather.40), kind=kOutput, calls=%fused_computation.38 | convolution fusion | flops 805502976 | bytes 7208960 | tf_op jit(solution)/shard_map/dot_general | solution.py:134
  128.3 3.5 %all-to-all-start.3 = ((bf16[4,384,128]{2,1,0:T(8,128)(2,1)}), bf16[4,384,128]{2,1,0:T(8,128)(2,1)S(1)}, u32[]{:S(2)}, u32[]{:S(2)}) async-start(bf16[4,384,128]{2,1,0:T(8,128)(2,1)} %bitcast.16), calls=%async_computation.3 | async-start | bytes 786432 | tf_op jit(solution)/shard_map/all_to_all | solution.py:141
  131.7 5.4 %convolution_convert_fusion = bf16[1536,128]{1,0:T(8,128)(2,1)} fusion(bf16[1536,2048]{1,0:T(8,128)(2,1)} %bitcast.1, bf16[2048,128]{1,0:T(8,128)(2,1)S(1)} %all_gather.42), kind=kOutput, calls=%fused_computation.36 | convolution fusion | flops 805502976 | bytes 7208960 | tf_op jit(solution)/shard_map/dot_general | solution.py:134
  137.1 5.4 %convolution_convert_fusion.1 = bf16[1536,128]{1,0:T(8,128)(2,1)} fusion(bf16[1536,2048]{1,0:T(8,128)(2,1)} %bitcast.1, bf16[2048,128]{1,0:T(8,128)(2,1)S(1)} %all_gather.41), kind=kOutput, calls=%fused_computation.37 | convolution fusion | flops 805502976 | bytes 7208960 | tf_op jit(solution)/shard_map/dot_general | solution.py:134
  142.5 4.2 %all-to-all-start.4 = ((bf16[4,384,128]{2,1,0:T(8,128)(2,1)}), bf16[4,384,128]{2,1,0:T(8,128)(2,1)S(1)}, u32[]{:S(2)}, u32[]{:S(2)}) async-start(bf16[4,384,128]{2,1,0:T(8,128)(2,1)} %bitcast.31), calls=%async_computation.4 | async-start | bytes 786432 | tf_op jit(solution)/shard_map/all_to_all | solution.py:141
  147.8 0.8 copy-done.2
  148.6 2.5 add_exponential_fusion
  151.1 1.4 all-to-all-done.4
  152.6 3.5 %all-to-all-start.5 = ((bf16[4,384,128]{2,1,0:T(8,128)(2,1)}), bf16[4,384,128]{2,1,0:T(8,128)(2,1)S(1)}, u32[]{:S(2)}, u32[]{:S(2)}) async-start(bf16[4,384,128]{2,1,0:T(8,128)(2,1)} %bitcast.34), calls=%async_computation.5 | async-start | bytes 786432 | tf_op jit(solution)/shard_map/all_to_all | solution.py:141
  156.2 2.2 copy.35
  158.4 1.8 fusion.52
  160.2 1.6 all-to-all-done.5
  161.9 2.3 bitcast_multiply_fusion.7
  164.1 20.6 %while.27 = (s32[]{:T(128)}, f32[4,128,128]{2,1,0:T(8,128)S(1)}, f32[6,4,64,128]{3,2,0,1:T(8,128)}, f32[6,4,64,128]{3,2,0,1:T(8,128)}, f32[6,4,64,128]{3,2,0,1:T...) while((s32[]{:T(128)}, f32[4,128,128]{2,1,0:T(8,128)S(1)}, ...), condition=%wide.region_4.5_spmd.clone, body=%wide.region_2.4_spmd.clone.sunk | while | flops 153575424 | bytes 3275900 | solution.py:79
  164.1 0.9 dynamic-slice_bitcast_fusion.2
  165.8 1.0 fusion.86
  166.9 0.7 convolution_add_fusion.5
  167.6 0.9 dynamic-slice_bitcast_fusion.2
  169.3 1.0 fusion.86
  171.0 0.9 dynamic-slice_bitcast_fusion.2
  172.7 1.0 fusion.86
  174.4 0.9 dynamic-slice_bitcast_fusion.2
  176.1 1.0 fusion.86
  177.9 0.9 dynamic-slice_bitcast_fusion.2
  179.6 1.0 fusion.86
  181.3 0.9 dynamic-slice_bitcast_fusion.2
  183.0 1.0 fusion.86
  184.7 0.7 copy-done.1
  185.5 0.9 constant_dynamic-slice_fusion.3
  186.4 0.9 constant_dynamic-slice_fusion.4
  187.3 19.7 %all_gather.38 = bf16[2048,128]{1,0:T(8,128)(2,1)S(1)} all-gather(bf16[512,128]{1,0:T(8,128)(2,1)S(1)} %constant_dynamic-slice_fusion.3), channel_id=1, replica_groups=mesh['sp'=4,'fs'=4,'tp'=2] {'sp'}, dimensions={0}, use_global_device_ids=true | all-gather | bytes 655360 | tf_op jit(solution)/shard_map/all_gather | solution.py:131
  207.0 20.7 %all_gather.37 = bf16[2048,128]{1,0:T(8,128)(2,1)S(1)} all-gather(bf16[512,128]{1,0:T(8,128)(2,1)S(1)} %constant_dynamic-slice_fusion.4), channel_id=1, replica_groups=mesh['sp'=4,'fs'=4,'tp'=2] {'sp'}, dimensions={0}, use_global_device_ids=true | all-gather | bytes 655360 | tf_op jit(solution)/shard_map/all_gather | solution.py:131
  227.7 4.6 %convolution_convert_fusion.3 = bf16[1536,128]{1,0:T(8,128)(2,1)S(1)} fusion(bf16[1536,2048]{1,0:T(8,128)(2,1)} %bitcast.1, bf16[2048,128]{1,0:T(8,128)(2,1)S(1)} %all_gather.38), kind=kOutput, calls=%fused_computation.39 | convolution fusion | flops 805502976 | bytes 7208960 | tf_op jit(solution)/shard_map/dot_general | solution.py:134
  232.3 1.0 copy.28
  233.3 3.5 %all-to-all-start.2 = ((bf16[4,384,128]{1,2,0:T(8,128)(2,1)}), bf16[4,384,128]{1,2,0:T(8,128)(2,1)S(1)}, u32[]{:S(2)}, u32[]{:S(2)}) async-start(bf16[4,384,128]{1,2,0:T(8,128)(2,1)} %copy.28), calls=%async_computation.2 | async-start | bytes 786432 | tf_op jit(solution)/shard_map/all_to_all | solution.py:141
  236.8 4.7 %convolution_convert_fusion.4 = bf16[1536,128]{1,0:T(8,128)(2,1)S(1)} fusion(bf16[1536,2048]{1,0:T(8,128)(2,1)} %bitcast.1, bf16[2048,128]{1,0:T(8,128)(2,1)S(1)} %all_gather.37), kind=kOutput, calls=%fused_computation.40 | convolution fusion | flops 805502976 | bytes 7208960 | tf_op jit(solution)/shard_map/dot_general | solution.py:134
  241.5 1.0 copy.27
  242.6 3.9 %all-to-all-start.1 = ((bf16[4,384,128]{1,2,0:T(8,128)(2,1)}), bf16[4,384,128]{1,2,0:T(8,128)(2,1)S(1)}, u32[]{:S(2)}, u32[]{:S(2)}) async-start(bf16[4,384,128]{1,2,0:T(8,128)(2,1)} %copy.27), calls=%async_computation.1 | async-start | bytes 786432 | tf_op jit(solution)/shard_map/all_to_all | solution.py:141
  247.6 1.3 collective-permute-start
  249.0 3.5 %all-to-all-done.1 = bf16[4,384,128]{1,2,0:T(8,128)(2,1)S(1)} async-done(((bf16[4,384,128]{1,2,0:T(8,128)(2,1)}), bf16[4,384,128]{1,2,0:T(8,128)(2,1)S(1)}, u32[]{:S(2)}, u32[]{:S(2)}) %all-to-all-start.1) | async-done | bytes 393248 | tf_op jit(solution)/shard_map/all_to_all | solution.py:141
  252.5 11.9 %all-gather.2 = f32[4,4,128]{2,1,0:T(4,128)S(1)} all-gather(f32[1,4,128]{2,1,0:T(4,128)S(1)} %bitcast.202), channel_id=2, replica_groups=mesh['sp'=4,'fs'=4,'tp'=2] {'sp'}, dimensions={0}, use_global_device_ids=true | all-gather | bytes 10240 | tf_op jit(solution)/shard_map/all_gather | solution.py:26
  264.8 0.7 fusion.50
  265.5 4.3 %fusion.54 = f32[384,2048]{1,0:T(8,128)} fusion(bf16[384,512]{0,1:T(8,128)(2,1)S(1)} %fusion.50, bf16[512,2048]{1,0:T(8,128)(2,1)} %all-gather.10.cloned.1.call-done), kind=kOutput, calls=%fused_computation.99 | convolution fusion | flops 805306368 | bytes 5636096 | tf_op jit(solution)/shard_map/dot_general | solution.py:185
  269.8 3.7 %while.28 = (s32[]{:T(128)}, f32[4,128,128]{2,1,0:T(8,128)S(1)}, s32[]{:T(128)}, f32[4,4,128]{2,1,0:T(4,128)S(1)}, f32[4,4,128,128]{3,2,1,0:T(8,128)}, /*index=5*/s32[]{:T(128)}, s32[]{:T(128)}) while((s32[]{:T(128)}, f32[4,128,128]{2,1,0:T(8,128)S(1)}, s32[]{:T(128)}, f32[4,4,128]{2,1,0:T(4,128)S(1)}, ...), condition=%wide.region_9.10_spmd.clone, body=%wide.region_8.9_spmd.clone.sunk | while | flops 262148 | bytes 792681 | solution.py:35
  269.8 1.2 fusion.87
  271.1 1.2 fusion.87
  272.3 1.1 fusion.87
  273.5 1.1 multiply_reduce_fusion
  274.8 8.6 %all-gather.12.cloned.1.call-done = bf16[512,2048]{1,0:T(8,128)(2,1)} async-done(((bf16[512,512]{1,0:T(8,128)(2,1)}), bf16[512,2048]{1,0:T(8,128)(2,1)}) %all-gather.12.cloned.1.call-update) | async-done | bytes 2097168 | tf_op jit(solution)/shard_map/all_gather | solution.py:182
  283.3 5.2 %convolution_add_fusion.2 = f32[384,2048]{1,0:T(8,128)} fusion(f32[384,2048]{1,0:T(8,128)} %fusion.54, bf16[384,512]{0,1:T(8,128)(2,1)S(1)} %bitcast.188, bf16[512,2048]{1,0:T(8,128)(2,1)} %all-gather.12.cloned.1.call-done), kind=kOutput, calls=%fused_computation.35 | convolution fusion | flops 806092800 | bytes 8781824 | tf_op jit(solution)/shard_map/dot_general | solution.py:186
  288.5 11.3 %reduce-scatter.2.cloned.1.call-done = f32[192,2048]{1,0:T(8,128)} async-done(((f32[384,2048]{1,0:T(8,128)}), f32[192,2048]{1,0:T(8,128)}) %reduce-scatter.2.cloned.1.call-update) | async-done | bytes 1572880 | tf_op jit(solution)/shard_map/reduce_scatter | solution.py:184
  299.9 2.4 convert_bitcast_fusion.2
  (97 shorter events, 11.6 us)
Async XLA Ops:
  7.4 28.8 %copy-start = (bf16[512,512]{1,0:T(8,128)(2,1)S(1)}, bf16[512,512]{1,0:T(8,128)(2,1)}, u32[]{:S(2)}) copy-start(bf16[512,512]{1,0:T(8,128)(2,1)} %param.22) | copy-start | bytes 1572868
  7.4 18.0 %all-gather.8.cloned.1.call-start = ((), (), s32[]{:S(2)}) async-start(), calls=%async_computation.7 | async-start | bytes 2359296 | tf_op jit(solution)/shard_map/all_gather | solution.py:113
  30.2 92.7 %all-to-all-start = ((bf16[4,1,384,2048]{3,2,1,0:T(8,128)(2,1)}), bf16[4,1,384,2048]{3,2,1,0:T(8,128)(2,1)}, u32[]{:S(2)}, u32[]{:S(2)}) async-start(bf16[4,1,384,2048]{3,2,1,0:T(8,128)(2,1)} %stack.3), calls=%async_computation | async-start | bytes 12582912 | tf_op jit(solution)/shard_map/all_to_all | solution.py:127
  35.5 50.7 %copy-start.6 = (f32[512]{0:T(512)S(1)}, f32[512]{0:T(512)}, u32[]{:S(2)}) copy-start(f32[512]{0:T(512)} %param.25) | copy-start | bytes 6148
  35.5 230.0 %all-gather.10.cloned.1.call-start = ((), (), s32[]{:S(2)}) async-start(), calls=%async_computation.8 | async-start | bytes 2621440 | tf_op jit(solution)/shard_map/all_gather | solution.py:181
  128.3 14.2 %all-to-all-start.3 = ((bf16[4,384,128]{2,1,0:T(8,128)(2,1)}), bf16[4,384,128]{2,1,0:T(8,128)(2,1)S(1)}, u32[]{:S(2)}, u32[]{:S(2)}) async-start(bf16[4,384,128]{2,1,0:T(8,128)(2,1)} %bitcast.16), calls=%async_computation.3 | async-start | bytes 786432 | tf_op jit(solution)/shard_map/all_to_all | solution.py:141
  137.1 9.5 %copy-start.5 = (f32[1,384,4]{1,2,0:T(4,128)S(1)}, f32[1,384,4]{1,2,0:T(4,128)}, u32[]{:S(2)}) copy-start(f32[1,384,4]{1,2,0:T(4,128)} %param.26) | copy-start | bytes 18436
  142.5 10.0 %all-to-all-start.4 = ((bf16[4,384,128]{2,1,0:T(8,128)(2,1)}), bf16[4,384,128]{2,1,0:T(8,128)(2,1)S(1)}, u32[]{:S(2)}, u32[]{:S(2)}) async-start(bf16[4,384,128]{2,1,0:T(8,128)(2,1)} %bitcast.31), calls=%async_computation.4 | async-start | bytes 786432 | tf_op jit(solution)/shard_map/all_to_all | solution.py:141
  147.5 1.0 copy-start.2
  152.6 9.3 %all-to-all-start.5 = ((bf16[4,384,128]{2,1,0:T(8,128)(2,1)}), bf16[4,384,128]{2,1,0:T(8,128)(2,1)S(1)}, u32[]{:S(2)}, u32[]{:S(2)}) async-start(bf16[4,384,128]{2,1,0:T(8,128)(2,1)} %bitcast.34), calls=%async_computation.5 | async-start | bytes 786432 | tf_op jit(solution)/shard_map/all_to_all | solution.py:141
  156.0 113.8 %all-gather.14.cloned.1.call-start = ((), (), s32[]{:S(2)}) async-start(), calls=%async_computation.11 | async-start | bytes 1310720 | tf_op jit(solution)/shard_map/all_gather | solution.py:26
  184.7 0.7 copy-start.1
  233.3 9.3 %all-to-all-start.2 = ((bf16[4,384,128]{1,2,0:T(8,128)(2,1)}), bf16[4,384,128]{1,2,0:T(8,128)(2,1)S(1)}, u32[]{:S(2)}, u32[]{:S(2)}) async-start(bf16[4,384,128]{1,2,0:T(8,128)(2,1)} %copy.28), calls=%async_computation.2 | async-start | bytes 786432 | tf_op jit(solution)/shard_map/all_to_all | solution.py:141
  236.8 10.4 %copy-start.8 = (f32[3,512]{1,0:T(4,128)S(1)}, f32[3,512]{1,0:T(4,128)}, u32[]{:S(2)}) copy-start(f32[3,512]{1,0:T(4,128)} %param.24) | copy-start | bytes 18436
  236.8 10.4 %copy-start.4 = (f32[6,4,64,128]{3,2,0,1:T(8,128)S(1)}, f32[6,4,64,128]{3,2,0,1:T(8,128)}, u32[]{:S(2)}) copy-start(f32[6,4,64,128]{3,2,0,1:T(8,128)} %get-tuple-element.142) | copy-start | bytes 2359300
  241.5 11.1 %copy-start.7 = (f32[4,128]{1,0:T(4,128)S(1)}, f32[4,128]{1,0:T(4,128)}, u32[]{:S(2)}) copy-start(f32[4,128]{1,0:T(4,128)} %get-tuple-element.227) | copy-start | bytes 6148
  242.6 9.8 %all-to-all-start.1 = ((bf16[4,384,128]{1,2,0:T(8,128)(2,1)}), bf16[4,384,128]{1,2,0:T(8,128)(2,1)S(1)}, u32[]{:S(2)}, u32[]{:S(2)}) async-start(bf16[4,384,128]{1,2,0:T(8,128)(2,1)} %copy.27), calls=%async_computation.1 | async-start | bytes 786432 | tf_op jit(solution)/shard_map/all_to_all | solution.py:141
  246.6 36.8 %all-gather.12.cloned.1.call-start = ((), (), s32[]{:S(2)}) async-start(), calls=%async_computation.9 | async-start | bytes 2621440 | tf_op jit(solution)/shard_map/all_gather | solution.py:182
  247.1 52.7 %reduce-scatter.2.cloned.1.call-start = ((), (), s32[]{:S(2)}) async-start(), calls=%async_computation.10 | async-start | bytes 4718592 | tf_op jit(solution)/shard_map/reduce_scatter | solution.py:184
  247.6 16.8 %collective-permute-start = (bf16[2,512]{0,1:T(8,128)(2,1)S(1)}, bf16[2,512]{0,1:T(8,128)(2,1)S(1)}, u32[]{:S(2)}, u32[]{:S(2)}) collective-permute-start(bf16[2,512]{0,1:T(8,128)(2,1)S(1)} %bitcast.196), channel_id=1, source_target_pairs={{0,8},{8,16},{16,24},{1,9},{9,17},{17,25},{2,10},{10,18},{18,26},{... | collective-permute-start | bytes 6152 | tf_op jit(solution)/shard_map/ppermute | solution.py:21
  269.8 3.7 %copy-start.3 = (f32[4,384,128]{2,1,0:T(8,128)S(1)}, f32[4,384,128]{2,1,0:T(8,128)}, u32[]{:S(2)}) copy-start(f32[4,384,128]{2,1,0:T(8,128)} %get-tuple-element.229) | copy-start | bytes 2359300
  269.8 4.8 %copy-start.9 = (f32[128]{0:T(128)S(1)}, f32[128]{0:T(128)}, u32[]{:S(2)}) copy-start(f32[128]{0:T(128)} %param.27) | copy-start | bytes 1540
Sparse Core Ops, SparseCore 0:
  12.9 12.5 all-gather.7
  288.7 11.1 reduce-scatter.1
Sparse Core Ops, SparseCore 1:
  37.8 76.3 all-gather.9
  185.6 39.6 all-gather.13
  248.9 34.4 all-gather.11
